TPU v7x, 512 devices: a whole 4x8x8 slice. The times are simulated.
512 devices in a mesh: ep: 128 (over z, y, core), tp: 4 (over x).
Axes of the slice: x: 4, y: 8, z: 8, core: 2. Of those that a mesh axis runs over, the one named last changes fastest.
Arguments:
- tokens: bfloat16 [2048, 2048], P('ep'), may hold values from -6 to 6
- head_state: float32 [2048, 16, 4096], P('ep', 'tp'), may hold values from -6 to 6
- mixer_gain: float32 [2048], replicated, may hold values from 0.1 to 1.9
- w_query: bfloat16 [2048, 1024], P('ep', 'tp'), may hold values from -0.125 to 0.125
- w_key: bfloat16 [2048, 1024], P('ep', 'tp'), may hold values from -0.125 to 0.125
- w_value: bfloat16 [2048, 1024], P('ep', 'tp'), may hold values from -0.125 to 0.125
- decay_down: bfloat16 [2048, 64], replicated, may hold values from -0.125 to 0.125
- decay_up: bfloat16 [64, 1024], replicated, may hold values from -3 to 3
- decay_base: float32 [1024], P('tp'), may hold values from -4 to 0
- rate_down: bfloat16 [2048, 64], replicated, may hold values from -0.125 to 0.125
- rate_up: bfloat16 [64, 1024], replicated, may hold values from -0.75 to 0.75
- head_gain: float32 [1024], P('tp'), may hold values from 0.1 to 1.9
- w_out: bfloat16 [1024, 2048], P('tp', 'ep'), may hold values from -0.1875 to 0.1875
- expert_gain: float32 [2048], replicated, may hold values from 0.1 to 1.9
- expert_ids: int32 [2048, 2], P('ep'), may hold values from 0 to 127, all different within a row; in each aligned block of 16 rows (0 to 15, 16 to 31, ...) at most 1 rows name the same one
- route_weight: float32 [2048, 2], P('ep'), may hold values from 0.2 to 1
- w_gate: bfloat16 [128, 2048, 512], P('ep', None, 'tp'), may hold values from -0.125 to 0.125
- w_up: bfloat16 [128, 2048, 512], P('ep', None, 'tp'), may hold values from -0.125 to 0.125
- w_down: bfloat16 [128, 512, 2048], P('ep', 'tp'), may hold values from -0.25 to 0.25
Outputs:
- layer_out: bfloat16 [2048, 2048], P('ep', 'tp')
- next_state: float32 [2048, 16, 4096], P('ep', 'tp')
Inputs may be any that keep to these rules, and one draw needn't show every extreme that they name: `expert_ids`: each row names 2 different experts; among the 16 rows of one index of ep no expert is named more than 1 times, and in the rows of some indices one expert is named exactly 1 times.
All inputs are finite; a program needn't handle non-finite values.
Results may differ from a plain program's by a relative error of at most 0.015.
Values may be sent and summed in bfloat16 or wider, within the bound.
A program may use at most 64 MiB of HBM per device.

v0:
```python
import jax
import jax.numpy as jnp
from jax import lax
from jax.sharding import PartitionSpec as P

norm_eps = 1e-06
group_eps = 0.00064


def sent_together(arrays, axis, dim, along):
    widths = [a.shape[along] for a in arrays]
    both = jnp.concatenate(arrays, axis=along)
    out = lax.all_gather(both, axis, axis=dim, tiled=True)
    return tuple(jnp.split(out, [sum(widths[:k]) for k in range(1, len(widths))], axis=along))


def from_everyone(array, axis):
    copies = jnp.broadcast_to(array, (lax.axis_size(axis), *array.shape))
    return lax.all_to_all(copies, axis, split_axis=0, concat_axis=0, tiled=True)


def taken_together(array, axis):
    everything = from_everyone(array, axis)
    return jnp.sum(everything.astype(jnp.float32), axis=0)


def split_up(array, dim, peers):
    before, after = (array.shape[:dim], array.shape[dim + 1 :])
    return jnp.moveaxis(array.reshape(*before, peers, -1, *after), dim, 0)


def sum_at_owner(array, axis, dim):
    peers = lax.axis_size(axis)
    parts = lax.all_to_all(split_up(array, dim, peers), axis, 0, 0, tiled=True)
    return jnp.sum(parts.astype(jnp.float32), axis=0)


def rms_scale(activity, gain):
    widened = activity.astype(jnp.float32)
    scaled = widened * lax.rsqrt(jnp.mean(widened * widened, axis=-1, keepdims=True) + norm_eps)
    return (scaled * gain).astype(jnp.bfloat16)


def low_rank(normed, decay_down, decay_up, decay_base, rate_down, rate_up):
    decay_low = jnp.tanh(jnp.dot(normed, decay_down, preferred_element_type=jnp.float32)).astype(
        jnp.bfloat16
    )
    decay_pre = decay_base + jnp.dot(decay_low, decay_up, preferred_element_type=jnp.float32)
    decays = jnp.exp(-jnp.exp(-jax.nn.softplus(-decay_pre) - 0.5))
    rate_low = jnp.dot(normed, rate_down, preferred_element_type=jnp.float32).astype(jnp.bfloat16)
    rates = jax.nn.sigmoid(jnp.dot(rate_low, rate_up, preferred_element_type=jnp.float32))
    return (decays, rates)


def recurrence(queries, key_rows, value_rows, decays, rates, old_state, head_gain):
    row_count, head_count, _ = old_state.shape
    head_size = queries.shape[1] // head_count
    head_shape = (row_count, head_count, head_size)
    query_heads = queries.astype(jnp.float32).reshape(head_shape)
    key_heads = key_rows.astype(jnp.float32).reshape(head_shape)
    value_heads = value_rows.astype(jnp.float32).reshape(head_shape)
    decay_heads = decays.reshape(head_shape)
    rate_heads = rates.reshape(head_shape)
    unit_keys = key_heads * lax.rsqrt(jnp.sum(key_heads * key_heads, axis=-1, keepdims=True) + 1.0)
    state_grid = old_state.reshape(row_count, head_count, head_size, head_size)
    removed = jnp.sum(state_grid * unit_keys[:, :, None, :], axis=-1)
    updated = (
        state_grid * decay_heads[:, :, None, :]
        - removed[:, :, :, None] * (unit_keys * rate_heads)[:, :, None, :]
        + value_heads[:, :, :, None] * key_heads[:, :, None, :]
    )
    readout = jnp.sum(updated * query_heads[:, :, None, :], axis=-1)
    centred = readout - jnp.mean(readout, axis=-1, keepdims=True)
    spread = jnp.mean(centred * centred, axis=-1, keepdims=True)
    scaled = centred * lax.rsqrt(spread + group_eps) * head_gain.reshape(head_count, head_size)
    return (
        updated.reshape(row_count, head_count, head_size * head_size),
        scaled.reshape(row_count, head_count * head_size).astype(jnp.bfloat16),
    )


def body(
    tokens,
    head_state,
    mixer_gain,
    w_query,
    w_key,
    w_value,
    decay_down,
    decay_up,
    decay_base,
    rate_down,
    rate_up,
    head_gain,
    w_out,
    expert_gain,
    expert_ids,
    route_weight,
    w_gate,
    w_up,
    w_down,
):
    seq_rows, width = tokens.shape
    local_cols = w_query.shape[1]
    head_lane = lax.axis_index("tp")
    normed = rms_scale(tokens, mixer_gain)
    pieces = sent_together((w_query, w_key, w_value), "ep", 0, 1)
    projected = tuple(
        (
            jnp.dot(normed, weight_piece, preferred_element_type=jnp.float32)
            for weight_piece in pieces
        )
    )
    queries, key_rows, value_rows = (member.astype(jnp.bfloat16) for member in projected)
    col_offset = head_lane * local_cols
    decays, rates = low_rank(
        normed,
        decay_down,
        lax.dynamic_slice_in_dim(decay_up, col_offset, local_cols, 1),
        decay_base,
        rate_down,
        lax.dynamic_slice_in_dim(rate_up, col_offset, local_cols, 1),
    )
    next_state, head_out = recurrence(
        queries, key_rows, value_rows, decays, rates, head_state, head_gain
    )
    partial_out = jnp.dot(
        head_out,
        lax.all_gather(w_out, "ep", axis=1, tiled=True),
        preferred_element_type=jnp.float32,
    )
    mixed_out = taken_together(partial_out.astype(jnp.bfloat16), "tp").astype(jnp.float32)
    residual = (tokens.astype(jnp.float32) + mixed_out).astype(jnp.bfloat16)
    expert_in = rms_scale(residual, expert_gain)
    experts = lax.axis_size("ep")
    top_count = expert_ids.shape[1]
    slot_count = max(1, 2 * seq_rows * top_count // experts)
    slot_total = experts * slot_count
    flat_ids = expert_ids.reshape(-1)
    matches = (flat_ids[:, None] == jnp.arange(experts, dtype=jnp.int32)[None, :]).astype(jnp.int32)
    slot_rank = jnp.sum((jnp.cumsum(matches, axis=0) - 1) * matches, axis=1)
    slot_ids = (flat_ids * slot_count + slot_rank).reshape(seq_rows, top_count)
    slot_match = (
        slot_ids[:, :, None] == jnp.arange(slot_total, dtype=jnp.int32)[None, None, :]
    ).astype(jnp.float32)
    picker = jnp.sum(slot_match, axis=1).astype(jnp.bfloat16)
    outbound = jnp.einsum("ts,td->sd", picker, expert_in, preferred_element_type=jnp.float32)
    outbound = outbound.astype(jnp.bfloat16).reshape(experts, slot_count, expert_in.shape[1])
    gate_local, up_local, down_local = (w_gate[0], w_up[0], w_down[0])
    arrived = lax.all_to_all(outbound, "ep", split_axis=0, concat_axis=0, tiled=True)
    sources, held, _ = arrived.shape
    flat_rows = arrived.reshape(sources * held, width)
    gate_act = jnp.dot(flat_rows, gate_local, preferred_element_type=jnp.float32)
    up_act = jnp.dot(flat_rows, up_local, preferred_element_type=jnp.float32)
    hidden = (jax.nn.silu(gate_act) * up_act).astype(jnp.bfloat16)
    partial_rows = jnp.dot(hidden, down_local, preferred_element_type=jnp.float32).reshape(
        sources, held, width
    )
    reduced = sum_at_owner(partial_rows.astype(jnp.bfloat16), "tp", 2)
    returned = lax.all_to_all(
        reduced.astype(jnp.bfloat16), "ep", split_axis=0, concat_axis=0, tiled=True
    )
    shares = route_weight / jnp.sum(route_weight, axis=1, keepdims=True)
    combine = jnp.sum(slot_match * shares[:, :, None], axis=1)
    routed = jnp.dot(combine, returned.reshape(slot_total, -1).astype(jnp.float32))
    own_cols = routed.shape[1]
    kept = lax.dynamic_slice_in_dim(residual, head_lane * own_cols, own_cols, 1)
    layer_out = (kept.astype(jnp.float32) + routed).astype(jnp.bfloat16)
    return (layer_out, next_state)


def solution(mesh):
    return jax.shard_map(
        body,
        mesh=mesh,
        in_specs=(
            P("ep", None),
            P("ep", "tp", None),
            P(),
            P("ep", "tp"),
            P("ep", "tp"),
            P("ep", "tp"),
            P(),
            P(),
            P("tp"),
            P(),
            P(),
            P("tp"),
            P("tp", "ep"),
            P(),
            P("ep", None),
            P("ep", None),
            P("ep", None, "tp"),
            P("ep", None, "tp"),
            P("ep", "tp", None),
        ),
        out_specs=(P("ep", "tp"), P("ep", "tp", None)),
        check_vma=False,
    )
```

profile of v0, /device:TPU:1, one launch (start us, length us, event | category | flops | bytes accessed | tf_op | source)
XLA Modules:
  0.0 267.5 jit_solution(1612568220506573948)
XLA Ops:
  7.2 1.4 pad_maximum_fusion
  8.7 0.7 all-gather.5.cloned.1.call-update
  9.4 1.0 fusion.34
  10.4 1.4 fusion.10
  11.8 1.4 fusion.55
  13.4 2.1 reshape.119
  15.5 1.5 mul.201
  17.0 3.1 %mul.221 = f32[16,4,4096]{2,1,0:T(4,128)} reshape(f32[16,4,64,64]{3,2,1,0:T(8,128)} %mul.201) | data formatting | bytes 2097152 | tf_op jit(solution)/shard_map/mul | solution.py:68
  20.2 0.1 eq.28
  20.4 80.8 %all-gather.3.cloned.1.call-done = bf16[2048,768]{1,0:T(8,128)(2,1)} async-done(((bf16[16,768]{1,0:T(8,128)(2,1)}), bf16[2048,768]{1,0:T(8,128)(2,1)}) %all-gather.3.cloned.1.call-update) | async-done | bytes 3145744 | tf_op jit(solution)/shard_map/all_gather | solution.py:13
  101.2 1.5 fusion.14
  102.8 1.5 fusion.12
  104.3 0.1 reshape.130
  104.4 1.5 fusion.13
  106.0 0.1 multiply_reduce_fusion.4
  106.2 8.8 %broadcast_multiply_fusion = (f32[16,4,64,64]{3,2,1,0:T(8,128)}, f32[16,4,64]{2,1,0:T(4,128)S(1)}, f32[16,4,64,64]{3,2,1,0:T(8,128)}) fusion(f32[16,4,64]{2,1,0:T(4,128)S(1)} %reshape.128, f32[16,4,64]{2,1,0:T(4,128)S(1)} %reshape.129, f32[16,4,64]{2,1,0:T(4,128)S(1)} %reshape.130, f32[16,4,64,64]{3,2,1,0:T(8,128)S(1)} %reshape.119, ...), kind=kOutput, calls=%fused_computation.33 | output fusion | flops 2097215 | bytes 3260416 | tf_op jit(solution)/shard_map/mul | solution.py:69
  115.1 3.2 %mul.223 = f32[16,4,4096]{2,1,0:T(4,128)} reshape(f32[16,4,64,64]{3,2,1,0:T(8,128)} %get-tuple-element.12) | data formatting | bytes 2097152 | tf_op jit(solution)/shard_map/mul | solution.py:69
  118.2 1.8 mul.224
  120.1 0.1 mul.219
  120.2 1.8 mul.225
  122.0 4.1 %multiply_reduce_fusion.2 = (f32[16,4]{1,0:T(8,128)S(1)}, f32[16,4,4096]{2,1,0:T(4,128)}) fusion(f32[16,4,4096]{2,1,0:T(4,128)} %mul.225, f32[16,4,4096]{2,1,0:T(4,128)} %mul.224, f32[16,4,4096]{2,1,0:T(4,128)} %mul.223, f32[16,4,4096]{2,1,0:T(4,128)} %param.20, f32[16,4,4096]{2,1,0:T(4,128)} %mul.221), kind=kLoop, calls=%fused_computation.31 | loop fusion | flops 1310656 | bytes 6291712 | tf_op jit(solution)/shard_map/reduce_sum | solution.py:73
  126.1 0.2 multiply_reduce_fusion.3
  126.3 0.1 subtract_multiply_fusion
  126.4 0.1 mul.230
  126.5 54.1 %all-gather.5.cloned.1.call-done = bf16[256,2048]{0,1:T(8,128)(2,1)} async-done(((bf16[256,16]{0,1:T(8,128)(2,1)}), bf16[256,2048]{0,1:T(8,128)(2,1)}) %all-gather.5.cloned.1.call-update) | async-done | bytes 1048592 | tf_op jit(solution)/shard_map/all_gather | solution.py:129
  180.6 1.6 convolution_convert_fusion.2
  182.2 0.7 broadcast_in_dim.2
  182.9 4.0 %all-to-all-start = ((bf16[4,16,2048]{2,1,0:T(8,128)(2,1)}), bf16[4,16,2048]{2,1,0:T(8,128)(2,1)S(1)}, u32[]{:S(2)}, u32[]{:S(2)}) async-start(bf16[4,16,2048]{2,1,0:T(8,128)(2,1)} %broadcast_in_dim.2), calls=%async_computation | async-start | bytes 524288 | tf_op jit(solution)/shard_map/all_to_all | solution.py:19
  186.9 0.2 select_reduce_fusion.1
  187.3 5.5 %all-to-all-done = bf16[4,16,2048]{2,1,0:T(8,128)(2,1)S(1)} async-done(((bf16[4,16,2048]{2,1,0:T(8,128)(2,1)}), bf16[4,16,2048]{2,1,0:T(8,128)(2,1)S(1)}, u32[]{:S(2)}, u32[]{:S(2)}) %all-to-all-start) | async-done | bytes 262176 | tf_op jit(solution)/shard_map/all_to_all | solution.py:19
  192.8 0.1 fusion.31
  193.0 0.3 fusion.1
  193.3 0.5 broadcast.118
  193.8 1.0 reduce.4
  194.9 0.4 reshape.132
  195.2 30.2 %all_to_all.20 = bf16[128,2,1024]{2,1,0:T(2,128)(2,1)S(1)} all-to-all(bf16[128,2,1024]{2,1,0:T(2,128)(2,1)S(1)} %reshape.132), channel_id=1, replica_groups=mesh['ep'=128,'tp'=4] {'ep'}, dimensions={0} | all-to-all | bytes 1048576 | tf_op jit(solution)/shard_map/all_to_all | solution.py:150
  225.4 0.4 reshape.133
  225.9 0.4 fusion.22
  226.3 0.7 convolution_convert_fusion
  227.0 0.4 reshape.125
  227.4 0.1 copy.85
  227.5 12.2 %all_to_all.21 = bf16[4,128,1,512]{3,1,2,0:T(8,128)(2,1)S(1)} all-to-all(bf16[4,128,1,512]{3,1,2,0:T(8,128)(2,1)S(1)} %bitcast.38), channel_id=1, replica_groups=mesh['ep'=128,'tp'=4] {'tp'}, dimensions={0} | all-to-all | bytes 1048576 | tf_op jit(solution)/shard_map/all_to_all | solution.py:34
  239.8 0.7 reduce.5
  240.5 0.7 reshape.134
  241.2 5.8 %all-to-all-start.3 = ((bf16[128,2,256]{2,1,0:T(2,128)(2,1)}), bf16[128,2,256]{2,1,0:T(2,128)(2,1)S(1)}, u32[]{:S(2)}, u32[]{:S(2)}) async-start(bf16[128,2,256]{2,1,0:T(2,128)(2,1)} %reshape.134), calls=%async_computation.3 | async-start | bytes 262144 | tf_op jit(solution)/shard_map/all_to_all | solution.py:160
  247.0 12.8 %all-to-all-done.3 = bf16[128,2,256]{2,1,0:T(2,128)(2,1)S(1)} async-done(((bf16[128,2,256]{2,1,0:T(2,128)(2,1)}), bf16[128,2,256]{2,1,0:T(2,128)(2,1)S(1)}, u32[]{:S(2)}, u32[]{:S(2)}) %all-to-all-start.3) | async-done | bytes 131104 | tf_op jit(solution)/shard_map/all_to_all | solution.py:160
  259.8 0.1 reshape.135
  259.9 0.8 fusion.7
  (44 shorter events, 1.2 us)
Async XLA Ops:
  7.2 219.2 %copy-start = (bf16[1,128,2048]{2,1,0:T(8,128)(2,1)S(1)}, bf16[1,128,2048]{2,1,0:T(8,128)(2,1)}, u32[]{:S(2)}) copy-start(bf16[1,128,2048]{2,1,0:T(8,128)(2,1)} %param.37) | copy-start | bytes 1572868
  7.2 94.0 %all-gather.3.cloned.1.call-start = ((), (), s32[]{:S(2)}) async-start(), calls=%async_computation.4 | async-start | bytes 3170304 | tf_op jit(solution)/shard_map/all_gather | solution.py:13
  8.6 172.0 %all-gather.5.cloned.1.call-start = ((), (), s32[]{:S(2)}) async-start(), calls=%async_computation.5 | async-start | bytes 1056768 | tf_op jit(solution)/shard_map/all_gather | solution.py:129
  17.0 3.1 %copy-start.7 = (s32[16,2]{0,1:T(2,128)S(1)}, s32[16,2]{0,1:T(2,128)}, u32[]{:S(2)}) copy-start(s32[16,2]{0,1:T(2,128)} %param.33) | copy-start | bytes 388
  17.0 3.4 %copy-start.8 = (f32[16,2]{0,1:T(2,128)S(1)}, f32[16,2]{0,1:T(2,128)}, u32[]{:S(2)}) copy-start(f32[16,2]{0,1:T(2,128)} %param.34) | copy-start | bytes 388
  17.0 84.2 %copy-start.2 = (bf16[16,2048]{1,0:T(8,128)(2,1)S(1)}, bf16[16,2048]{1,0:T(8,128)(2,1)}, u32[]{:S(2)}) copy-start(bf16[16,2048]{1,0:T(8,128)(2,1)} %param.19) | copy-start | bytes 196612
  17.0 84.2 %copy-start.5 = (f32[2048]{0:T(1024)S(1)}, f32[2048]{0:T(1024)}, u32[]{:S(2)}) copy-start(f32[2048]{0:T(1024)} %param.21) | copy-start | bytes 24580
  115.1 3.2 %copy-start.1 = (f32[16,4,64,64]{3,2,1,0:T(8,128)S(1)}, f32[16,4,64,64]{3,2,1,0:T(8,128)}, u32[]{:S(2)}) copy-start(f32[16,4,64,64]{3,2,1,0:T(8,128)} %get-tuple-element.10) | copy-start | bytes 3145732
  122.0 58.6 %copy-start.9 = (f32[256]{0:T(256)S(1)}, f32[256]{0:T(256)}, u32[]{:S(2)}) copy-start(f32[256]{0:T(256)} %param.30) | copy-start | bytes 3076
  126.1 66.8 %copy-start.6 = (f32[2048]{0:T(1024)S(1)}, f32[2048]{0:T(1024)}, u32[]{:S(2)}) copy-start(f32[2048]{0:T(1024)} %param.32) | copy-start | bytes 24580
  182.9 9.9 %all-to-all-start = ((bf16[4,16,2048]{2,1,0:T(8,128)(2,1)}), bf16[4,16,2048]{2,1,0:T(8,128)(2,1)S(1)}, u32[]{:S(2)}, u32[]{:S(2)}) async-start(bf16[4,16,2048]{2,1,0:T(8,128)(2,1)} %broadcast_in_dim.2), calls=%async_computation | async-start | bytes 524288 | tf_op jit(solution)/shard_map/all_to_all | solution.py:19
  194.8 31.1 %copy-start.3 = (bf16[1,2048,128]{2,1,0:T(8,128)(2,1)S(1)}, bf16[1,2048,128]{2,1,0:T(8,128)(2,1)}, u32[]{:S(2)}) copy-start(bf16[1,2048,128]{2,1,0:T(8,128)(2,1)} %param.35) | copy-start | bytes 1572868
  195.2 31.1 %copy-start.4 = (bf16[1,2048,128]{2,1,0:T(8,128)(2,1)S(1)}, bf16[1,2048,128]{2,1,0:T(8,128)(2,1)}, u32[]{:S(2)}) copy-start(bf16[1,2048,128]{2,1,0:T(8,128)(2,1)} %param.36) | copy-start | bytes 1572868
  241.2 18.6 %all-to-all-start.3 = ((bf16[128,2,256]{2,1,0:T(2,128)(2,1)}), bf16[128,2,256]{2,1,0:T(2,128)(2,1)S(1)}, u32[]{:S(2)}, u32[]{:S(2)}) async-start(bf16[128,2,256]{2,1,0:T(2,128)(2,1)} %reshape.134), calls=%async_computation.3 | async-start | bytes 262144 | tf_op jit(solution)/shard_map/all_to_all | solution.py:160
Sparse Core Ops, SparseCore 0:
  11.7 89.4 all-gather.2
  104.2 76.3 all-gather.4
where the time goes:
time: 268 us; the launch traced here: 267 us
  waiting for transfers between devices  154 us (57%)
  blocking collectives  42.4 us (16%)
  other arithmetic  18.1 us (7%)
  local copies, waits for them, and re-layouts  17.9 us (7%)
  between operations  14.3 us (5%)
  matrix products  11.1 us (4%)
  starting transfers between devices  9.82 us (4%)
    all_gather x1, waiting for transfers between devices, sent_together(): out = lax.all_gather(both, axis, axis=dim, tiled=True)  80.8 us
    all_gather x1, waiting for transfers between devices, body(): lax.all_gather(w_out, 'ep', axis=1, tiled=True)  54.1 us
    all_to_all x1, blocking collectives, body(): lax.all_to_all(outbound, 'ep', split_axis=0, concat_axis=0, tiled=True)  30.2 us
    all_to_all x1, waiting for transfers between devices, body(): lax.all_to_all(reduced.astype(jnp.bfloat16), 'ep', split_axis=0, concat_a...  12.8 us
    all_to_all x1, blocking collectives, sum_at_owner(): parts = lax.all_to_all(split_up(array, dim, peers), axis, 0, 0, tiled=True)  12.2 us
    mul x1, other arithmetic, recurrence(): removed[:, :, :, None] * (unit_keys * rate_heads)[:, :, None, :]  8.83 us
    all_to_all x1, starting transfers between devices, body(): lax.all_to_all(reduced.astype(jnp.bfloat16), 'ep', split_axis=0, concat_a...  5.77 us
    all_to_all x1, waiting for transfers between devices, from_everyone(): return lax.all_to_all(copies, axis, split_axis=0, concat_axis=0, tiled=True)  5.47 us
  transfers between devices with their start and end apart: 4, of which 4 were waited for; matrix products, arithmetic and copies ran while one was open for 14% of the time, Pallas kernels for 0%

commit v1 on v0

--- a/solution.py
+++ b/solution.py
@@ -1,10 +1,144 @@
 import jax
 import jax.numpy as jnp
 from jax import lax
+from jax.experimental import pallas as pl
+from jax.experimental.pallas import tpu as pltpu
 from jax.sharding import PartitionSpec as P
 
 norm_eps = 1e-06
 group_eps = 0.00064
+
+MESH = pl.DeviceIdType.MESH
+
+
+def offset_at(i):
+    return ((i + 1) // 2) * (2 * (i % 2) - 1)
+
+
+def gather_kernel(wq, wk, wv, wo, out, own_sem, send_sem, recv_sem):
+    ep = lax.axis_index("ep")
+    core = ep % 2
+    y = (ep // 2) % 8
+    z = ep // 16
+    a = z + core * (y - z)
+    b = y + core * (z - y)
+    partner = ep + 1 - 2 * core
+
+    def at(da, db):
+        aa = (a + da + 8) % 8
+        bb = (b + db + 8) % 8
+        return aa * (16 - 14 * core) + bb * (2 + 14 * core) + core
+
+    barrier = pltpu.get_barrier_semaphore()
+    for i in range(1, 8):
+        pl.semaphore_signal(barrier, inc=1, device_id={"ep": at(offset_at(i), 0)}, device_id_type=MESH)
+    pl.semaphore_signal(barrier, inc=1, device_id={"ep": at(0, 1)}, device_id_type=MESH)
+    pl.semaphore_signal(barrier, inc=1, device_id={"ep": at(0, -1)}, device_id_type=MESH)
+    pl.semaphore_signal(barrier, inc=1, device_id={"ep": partner}, device_id_type=MESH)
+
+    own = [
+        pltpu.make_async_copy(w, out.at[m, ep], own_sem.at[m]) for m, w in enumerate((wq, wk, wv, wo))
+    ]
+    for copy in own:
+        copy.start()
+    for copy in own:
+        copy.wait()
+    pl.semaphore_wait(barrier, 10)
+
+    def copy_of(block, slot, to):
+        return pltpu.make_async_remote_copy(
+            src_ref=out.at[:, block],
+            dst_ref=out.at[:, block],
+            send_sem=send_sem.at[slot],
+            recv_sem=recv_sem.at[block],
+            device_id={"ep": to},
+            device_id_type=MESH,
+        )
+
+    def send(block, slot, to):
+        copy_of(block, slot, to).start()
+
+    def arrived(block):
+        copy_of(block, 0, partner).wait_recv()
+
+    forth = at(0, 1)
+    back = at(0, -1)
+
+    @pl.loop(1, 8)
+    def _(i):
+        send(ep, i, at(offset_at(i), 0))
+
+    @pl.loop(0, 8)
+    def _(i):
+        block = at(offset_at(i), 0)
+
+        @pl.when(i > 0)
+        def _():
+            arrived(block)
+
+        send(block, 8 + i, forth)
+        send(block, 36 + i, back)
+        send(block, 64 + i, partner)
+
+    @pl.loop(1, 3)
+    def _(s):
+        @pl.loop(0, 8)
+        def _(i):
+            o = offset_at(i)
+            left = at(o, -s)
+            arrived(left)
+            send(left, 8 + 8 * s + i, forth)
+            send(left, 64 + 16 * s - 8 + i, partner)
+            right = at(o, s)
+            arrived(right)
+            send(right, 36 + 8 * s + i, back)
+            send(right, 64 + 16 * s + i, partner)
+
+    @pl.loop(0, 4)
+    def _(h):
+        for d in range(2):
+            i = 2 * h + d
+            o = offset_at(i)
+            left = at(o, -3)
+            arrived(left)
+            if d == 0:
+                send(left, 8 + 24 + h, forth)
+            send(left, 64 + 40 + i, partner)
+            right = at(o, 3)
+            arrived(right)
+            if d == 1:
+                send(right, 36 + 24 + h, back)
+            send(right, 64 + 48 + i, partner)
+
+    @pl.loop(0, 8)
+    def _(i):
+        block = at(offset_at(i), 4)
+        arrived(block)
+        send(block, 64 + 56 + i, partner)
+
+    @pl.loop(0, 64)
+    def _(k):
+        arrived(2 * k + 1 - core)
+
+    @pl.loop(1, 128)
+    def _(k):
+        copy_of(ep, k, partner).wait_send()
+
+
+def gather_weights(w_query, w_key, w_value, w_out_t):
+    rows, cols = w_query.shape
+    return pl.pallas_call(
+        gather_kernel,
+        out_shape=jax.ShapeDtypeStruct((4, 128, rows, cols), jnp.bfloat16),
+        in_specs=[pl.BlockSpec(memory_space=pl.ANY)] * 4,
+        out_specs=pl.BlockSpec(memory_space=pltpu.VMEM),
+        scratch_shapes=[
+            pltpu.SemaphoreType.DMA((4,)),
+            pltpu.SemaphoreType.DMA((128,)),
+            pltpu.SemaphoreType.DMA((128,)),
+        ],
+        compiler_params=pltpu.CompilerParams(collective_id=0, has_side_effects=True),
+    )(w_query, w_key, w_value, w_out_t)
 
 
 def sent_together(arrays, axis, dim, along):
@@ -104,7 +238,9 @@
     local_cols = w_query.shape[1]
     head_lane = lax.axis_index("tp")
     normed = rms_scale(tokens, mixer_gain)
-    pieces = sent_together((w_query, w_key, w_value), "ep", 0, 1)
+    gathered = gather_weights(w_query, w_key, w_value, w_out.T)
+    full = gathered.reshape(4, width, local_cols)
+    pieces = (full[0], full[1], full[2])
     projected = tuple(
         (
             jnp.dot(normed, weight_piece, preferred_element_type=jnp.float32)
@@ -124,10 +260,8 @@
     next_state, head_out = recurrence(
         queries, key_rows, value_rows, decays, rates, head_state, head_gain
     )
-    partial_out = jnp.dot(
-        head_out,
-        lax.all_gather(w_out, "ep", axis=1, tiled=True),
-        preferred_element_type=jnp.float32,
+    partial_out = lax.dot_general(
+        head_out, full[3], (((1,), (1,)), ((), ())), preferred_element_type=jnp.float32
     )
     mixed_out = taken_together(partial_out.astype(jnp.bfloat16), "tp").astype(jnp.float32)
     residual = (tokens.astype(jnp.float32) + mixed_out).astype(jnp.bfloat16)

time: 268 us -> 155 us (0.58)
  waiting for transfers between devices: 154 us -> 18.9 us
  Pallas kernels: 0 us -> 40.6 us
  between operations: 14.3 us -> 0.97 us
  matrix products: 11.1 us -> 5.95 us
    all_gather x2 -> x0, waiting for transfers between devices: 135 us -> none  [the longest x1 80.8 us: sent_together(): out = lax.all_gather(both, axis, axis=dim, tiled=True)]
    pallas_call x0 -> x1, Pallas kernels: none -> 40.6 us  [gather_weights(): pl.pallas_call(gather_kernel, out_shape=jax.ShapeDtypeStruct((4, 128, row...]
    dot_general x3, matrix products: 4.53 us -> 0.86 us  [body(): jnp.dot(normed, weight_piece, preferred_element_type=jnp.float32)]
    slice x0 -> x1, local copies, waits for them, and re-layouts: none -> 3.59 us  [body(): full[3]]
  transfers between devices with their start and end apart: 4 -> 2, of which waited for: 4 -> 2; matrix products, arithmetic and copies ran while one was open for 14% -> 0% of each run, Pallas kernels for 0% -> 0%
where the time goes in v1:
time: 155 us
  blocking collectives  42.5 us (27%)
  Pallas kernels  40.6 us (26%)
  local copies, waits for them, and re-layouts  19 us (12%)
  waiting for transfers between devices  18.9 us (12%)
  other arithmetic  16.8 us (11%)
  starting transfers between devices  9.79 us (6%)
  matrix products  5.95 us (4%)
    pallas_call x1, Pallas kernels, gather_weights(): pl.pallas_call(gather_kernel, out_shape=jax.ShapeDtypeStruct((4, 128, row...  40.6 us
    all_to_all x1, blocking collectives, body(): lax.all_to_all(outbound, 'ep', split_axis=0, concat_axis=0, tiled=True)  30.2 us
    all_to_all x1, waiting for transfers between devices, body(): lax.all_to_all(reduced.astype(jnp.bfloat16), 'ep', split_axis=0, concat_a...  12.8 us
    all_to_all x1, blocking collectives, sum_at_owner(): parts = lax.all_to_all(split_up(array, dim, peers), axis, 0, 0, tiled=True)  12.2 us
    mul x1, other arithmetic, recurrence(): removed[:, :, :, None] * (unit_keys * rate_heads)[:, :, None, :]  8.83 us
    all_to_all x1, waiting for transfers between devices, from_everyone(): return lax.all_to_all(copies, axis, split_axis=0, concat_axis=0, tiled=True)  6.12 us
    all_to_all x1, starting transfers between devices, body(): lax.all_to_all(reduced.astype(jnp.bfloat16), 'ep', split_axis=0, concat_a...  5.77 us
    reduce_sum x1, other arithmetic, recurrence(): centred = readout - jnp.mean(readout, axis=-1, keepdims=True)  4.18 us
  transfers between devices with their start and end apart: 2, of which 2 were waited for; matrix products, arithmetic and copies ran while one was open for 0% of the time, Pallas kernels for 0%

profile of v1, /device:TPU:1, one launch (start us, length us, event | category | flops | bytes accessed | tf_op | source)
XLA Modules:
  0.0 154.5 jit_solution(419057785754645804)
XLA Ops:
  0.6 1.0 fusion.31
  1.7 1.4 fusion.10
  3.2 40.6 %shard_map.194 = bf16[4,128,16,256]{3,2,1,0:T(8,128)(2,1)} custom-call(bf16[16,256]{1,0:T(8,128)(2,1)} %wq.1, bf16[16,256]{1,0:T(8,128)(2,1)} %wk.1, bf16[16,256]{1,0:T(8,128)(2,1)} %wv.1, bf16[16,256]{1,0:T(8,128)(2,1)} %bitcast.53), custom_call_target="tpu_custom_call" | custom-call | tf_op jit(solution)/shard_map/pallas_call | solution.py:130
  43.8 3.6 %fusion.69 = (bf16[1,128,16,256]{3,2,1,0:T(8,128)(2,1)}, bf16[1,128,16,256]{3,2,1,0:T(8,128)(2,1)S(1)}, bf16[1,128,16,256]{3,2,1,0:T(8,128)(2,1)S(1)}, bf16[1,128,16,256]{3,2,1,0:T(8,128)(2,1)S(1)}) fusion(bf16[4,128,16,256]{3,2,1,0:T(8,128)(2,1)} %shard_map.194), kind=kLoop, calls=%fused_computation.93 | loop fusion | bytes 8388608 | tf_op jit(solution)/shard_map/slice | solution.py:264
  47.4 0.3 fusion.14
  47.7 0.1 reshape.174
  47.8 0.1 multiply_reduce_fusion.4
  47.9 1.2 fusion.52
  49.2 0.3 fusion.12
  49.5 0.1 reshape.176
  49.5 0.3 fusion.13
  49.9 2.1 %reshape.165 = f32[16,4,64,64]{3,2,1,0:T(8,128)S(1)} reshape(f32[16,4,4096]{2,1,0:T(4,128)} %param.20) | data formatting | bytes 2097152 | tf_op jit(solution)/shard_map/reshape | solution.py:199
  52.2 8.8 %broadcast_multiply_fusion = (f32[16,4,64,64]{3,2,1,0:T(8,128)}, f32[16,4,64]{2,1,0:T(4,128)S(1)}, f32[16,4,64,64]{3,2,1,0:T(8,128)}) fusion(f32[16,4,64]{2,1,0:T(4,128)S(1)} %reshape.174, f32[16,4,64]{2,1,0:T(4,128)S(1)} %reshape.175, f32[16,4,64]{2,1,0:T(4,128)S(1)} %reshape.176, f32[16,4,64,64]{3,2,1,0:T(8,128)S(1)} %reshape.165, ...), kind=kOutput, calls=%fused_computation.30 | output fusion | flops 2097215 | bytes 3260416 | tf_op jit(solution)/shard_map/mul | solution.py:203
  61.0 3.2 %mul.236 = f32[16,4,4096]{2,1,0:T(4,128)} reshape(f32[16,4,64,64]{3,2,1,0:T(8,128)} %get-tuple-element.16) | data formatting | bytes 2097152 | tf_op jit(solution)/shard_map/mul | solution.py:203
  64.2 1.8 %mul.237 = f32[16,4,4096]{2,1,0:T(4,128)} reshape(f32[16,4,64,64]{3,2,1,0:T(8,128)S(1)} %copy-done.1) | data formatting | bytes 2097152 | tf_op jit(solution)/shard_map/mul | solution.py:204
  66.0 0.1 mul.214
  66.1 1.9 %mul.234 = f32[16,4,4096]{2,1,0:T(4,128)} reshape(f32[16,4,64,64]{3,2,1,0:T(8,128)S(1)} %mul.214) | data formatting | bytes 2097152 | tf_op jit(solution)/shard_map/mul | solution.py:202
  68.0 0.1 mul.232
  68.2 1.8 %mul.238 = f32[16,4,4096]{2,1,0:T(4,128)} reshape(f32[16,4,64,64]{3,2,1,0:T(8,128)S(1)} %mul.232) | data formatting | bytes 2097152 | tf_op jit(solution)/shard_map/mul | solution.py:206
  70.0 4.2 %multiply_reduce_fusion.2 = (f32[16,4]{1,0:T(8,128)S(1)}, f32[16,4,4096]{2,1,0:T(4,128)}) fusion(f32[16,4,4096]{2,1,0:T(4,128)} %mul.238, f32[16,4,4096]{2,1,0:T(4,128)} %mul.237, f32[16,4,4096]{2,1,0:T(4,128)} %mul.236, f32[16,4,4096]{2,1,0:T(4,128)} %param.20, f32[16,4,4096]{2,1,0:T(4,128)} %mul.234), kind=kLoop, calls=%fused_computation.28 | loop fusion | flops 1310656 | bytes 6291712 | tf_op jit(solution)/shard_map/reduce_sum | solution.py:207
  74.2 0.2 multiply_reduce_fusion.3
  74.4 0.1 multiply_convert_fusion
  74.5 0.1 convert_element_type.88
  74.6 0.4 convolution_convert_fusion.2
  75.0 0.7 broadcast_in_dim.2
  75.7 4.0 %all-to-all-start = ((bf16[4,16,2048]{2,1,0:T(8,128)(2,1)}), bf16[4,16,2048]{2,1,0:T(8,128)(2,1)S(1)}, u32[]{:S(2)}, u32[]{:S(2)}) async-start(bf16[4,16,2048]{2,1,0:T(8,128)(2,1)} %broadcast_in_dim.2), calls=%async_computation | async-start | bytes 524288 | tf_op jit(solution)/shard_map/all_to_all | solution.py:153
  79.8 0.1 eq.28
  80.1 0.2 select_reduce_fusion.1
  80.4 0.1 copy.64
  80.5 6.1 %all-to-all-done = bf16[4,16,2048]{2,1,0:T(8,128)(2,1)S(1)} async-done(((bf16[4,16,2048]{2,1,0:T(8,128)(2,1)}), bf16[4,16,2048]{2,1,0:T(8,128)(2,1)S(1)}, u32[]{:S(2)}, u32[]{:S(2)}) %all-to-all-start) | async-done | bytes 262176 | tf_op jit(solution)/shard_map/all_to_all | solution.py:153
  86.7 0.1 fusion.28
  86.8 0.3 fusion.1
  87.2 0.5 broadcast.134
  87.7 1.0 reduce.4
  88.7 0.4 reshape.178
  89.1 30.2 %all_to_all.20 = bf16[128,2,1024]{2,1,0:T(2,128)(2,1)S(1)} all-to-all(bf16[128,2,1024]{2,1,0:T(2,128)(2,1)S(1)} %reshape.178), channel_id=1, replica_groups=mesh['ep'=128,'tp'=4] {'ep'}, dimensions={0} | all-to-all | bytes 1048576 | tf_op jit(solution)/shard_map/all_to_all | solution.py:284
  119.3 0.4 reshape.179
  119.8 0.4 fusion.19
  120.2 0.7 convolution_convert_fusion
  120.9 0.4 reshape.171
  121.3 0.1 copy.85
  121.4 12.2 %all_to_all.21 = bf16[4,128,1,512]{3,1,2,0:T(8,128)(2,1)S(1)} all-to-all(bf16[4,128,1,512]{3,1,2,0:T(8,128)(2,1)S(1)} %bitcast.51), channel_id=1, replica_groups=mesh['ep'=128,'tp'=4] {'tp'}, dimensions={0} | all-to-all | bytes 1048576 | tf_op jit(solution)/shard_map/all_to_all | solution.py:168
  133.7 0.7 reduce.5
  134.4 0.7 reshape.180
  135.1 5.8 %all-to-all-start.3 = ((bf16[128,2,256]{2,1,0:T(2,128)(2,1)}), bf16[128,2,256]{2,1,0:T(2,128)(2,1)S(1)}, u32[]{:S(2)}, u32[]{:S(2)}) async-start(bf16[128,2,256]{2,1,0:T(2,128)(2,1)} %reshape.180), calls=%async_computation.3 | async-start | bytes 262144 | tf_op jit(solution)/shard_map/all_to_all | solution.py:294
  140.9 12.8 %all-to-all-done.3 = bf16[128,2,256]{2,1,0:T(2,128)(2,1)S(1)} async-done(((bf16[128,2,256]{2,1,0:T(2,128)(2,1)}), bf16[128,2,256]{2,1,0:T(2,128)(2,1)S(1)}, u32[]{:S(2)}, u32[]{:S(2)}) %all-to-all-start.3) | async-done | bytes 131104 | tf_op jit(solution)/shard_map/all_to_all | solution.py:294
  153.7 0.1 reshape.181
  153.8 0.8 fusion.7
  (46 shorter events, 1.0 us)
Async XLA Ops:
  0.6 119.6 %copy-start = (bf16[1,128,2048]{2,1,0:T(8,128)(2,1)S(1)}, bf16[1,128,2048]{2,1,0:T(8,128)(2,1)}, u32[]{:S(2)}) copy-start(bf16[1,128,2048]{2,1,0:T(8,128)(2,1)} %param.37) | copy-start | bytes 1572868
  43.8 3.6 %copy-start.3 = (bf16[16,2048]{1,0:T(8,128)(2,1)S(1)}, bf16[16,2048]{1,0:T(8,128)(2,1)}, u32[]{:S(2)}) copy-start(bf16[16,2048]{1,0:T(8,128)(2,1)} %param.19) | copy-start | bytes 196612
  43.8 3.6 %copy-start.7 = (f32[2048]{0:T(1024)S(1)}, f32[2048]{0:T(1024)}, u32[]{:S(2)}) copy-start(f32[2048]{0:T(1024)} %param.21) | copy-start | bytes 24580
  43.8 4.1 %copy-start.6 = (bf16[2048,64]{0,1:T(8,128)(2,1)S(1)}, bf16[2048,64]{0,1:T(8,128)(2,1)}, u32[]{:S(2)}) copy-start(bf16[2048,64]{0,1:T(8,128)(2,1)} %param.25) | copy-start | bytes 786436
  43.8 4.1 %copy-start.11 = (f32[256]{0:T(256)S(1)}, f32[256]{0:T(256)}, u32[]{:S(2)}) copy-start(f32[256]{0:T(256)} %param.27) | copy-start | bytes 3076
  61.0 3.2 %copy-start.1 = (f32[16,4,64,64]{3,2,1,0:T(8,128)S(1)}, f32[16,4,64,64]{3,2,1,0:T(8,128)}, u32[]{:S(2)}) copy-start(f32[16,4,64,64]{3,2,1,0:T(8,128)} %get-tuple-element.14) | copy-start | bytes 3145732
  70.0 4.4 %copy-start.12 = (f32[256]{0:T(256)S(1)}, f32[256]{0:T(256)}, u32[]{:S(2)}) copy-start(f32[256]{0:T(256)} %param.30) | copy-start | bytes 3076
  70.0 4.7 %copy-start.2 = (bf16[1,128,16,256]{3,2,1,0:T(8,128)(2,1)S(1)}, bf16[1,128,16,256]{3,2,1,0:T(8,128)(2,1)}, u32[]{:S(2)}) copy-start(bf16[1,128,16,256]{3,2,1,0:T(8,128)(2,1)} %get-tuple-element.10) | copy-start | bytes 3145732
  74.2 5.6 %copy-start.9 = (s32[16,2]{0,1:T(2,128)S(1)}, s32[16,2]{0,1:T(2,128)}, u32[]{:S(2)}) copy-start(s32[16,2]{0,1:T(2,128)} %param.33) | copy-start | bytes 388
  74.2 5.9 %copy-start.10 = (f32[16,2]{0,1:T(2,128)S(1)}, f32[16,2]{0,1:T(2,128)}, u32[]{:S(2)}) copy-start(f32[16,2]{0,1:T(2,128)} %param.34) | copy-start | bytes 388
  74.2 12.7 %copy-start.8 = (f32[2048]{0:T(1024)S(1)}, f32[2048]{0:T(1024)}, u32[]{:S(2)}) copy-start(f32[2048]{0:T(1024)} %param.32) | copy-start | bytes 24580
  75.7 10.9 %all-to-all-start = ((bf16[4,16,2048]{2,1,0:T(8,128)(2,1)}), bf16[4,16,2048]{2,1,0:T(8,128)(2,1)S(1)}, u32[]{:S(2)}, u32[]{:S(2)}) async-start(bf16[4,16,2048]{2,1,0:T(8,128)(2,1)} %broadcast_in_dim.2), calls=%async_computation | async-start | bytes 524288 | tf_op jit(solution)/shard_map/all_to_all | solution.py:153
  88.7 31.1 %copy-start.4 = (bf16[1,2048,128]{2,1,0:T(8,128)(2,1)S(1)}, bf16[1,2048,128]{2,1,0:T(8,128)(2,1)}, u32[]{:S(2)}) copy-start(bf16[1,2048,128]{2,1,0:T(8,128)(2,1)} %param.35) | copy-start | bytes 1572868
  89.1 31.2 %copy-start.5 = (bf16[1,2048,128]{2,1,0:T(8,128)(2,1)S(1)}, bf16[1,2048,128]{2,1,0:T(8,128)(2,1)}, u32[]{:S(2)}) copy-start(bf16[1,2048,128]{2,1,0:T(8,128)(2,1)} %param.36) | copy-start | bytes 1572868
  135.1 18.6 %all-to-all-start.3 = ((bf16[128,2,256]{2,1,0:T(2,128)(2,1)}), bf16[128,2,256]{2,1,0:T(2,128)(2,1)S(1)}, u32[]{:S(2)}, u32[]{:S(2)}) async-start(bf16[128,2,256]{2,1,0:T(2,128)(2,1)} %reshape.180), calls=%async_computation.3 | async-start | bytes 262144 | tf_op jit(solution)/shard_map/all_to_all | solution.py:294
